TPU v7x, 32 devices: a whole 2x2x4 slice. The times are simulated.
32 devices in a mesh: fs: 8 (over z, x), tp: 4 (over y, core).
Axes of the slice: x: 2, y: 2, z: 4, core: 2. Of those that a mesh axis runs over, the one named last changes fastest.
Arguments:
- tokens: bfloat16 [1536, 2048], P('fs'), may hold values from -6 to 6
- norm_gain: float32 [2048], P('fs'), may hold values from 0.1 to 1.9
- expert_gate: float32 [16, 2048, 1024], P(None, 'fs', 'tp'), may hold values from -0.125 to 0.125
- expert_up: float32 [16, 2048, 1024], P(None, 'fs', 'tp'), may hold values from -0.125 to 0.125
- expert_down: float32 [16, 1024, 2048], P(None, 'fs', 'tp'), may hold values from -0.1875 to 0.1875
- shared_gate: float32 [2048, 1024], P('fs', 'tp'), may hold values from -0.125 to 0.125
- shared_up: float32 [2048, 1024], P('fs', 'tp'), may hold values from -0.125 to 0.125
- shared_down: float32 [1024, 2048], P('fs', 'tp'), may hold values from -0.1875 to 0.1875
- expert_ids: int32 [1536, 8], P('fs'), may hold values from 0 to 15, all different within a row; in each aligned block of 192 rows (0 to 191, 192 to 383, ...) at most 192 rows name the same one
- route_weights: float32 [1536, 8], P('fs'), may hold values from 0.25 to 1
Outputs:
- gate_ready: bfloat16 [16, 2048, 1024], P('fs', None, 'tp')
- up_ready: bfloat16 [16, 2048, 1024], P('fs', None, 'tp')
- down_ready: bfloat16 [16, 1024, 2048], P('fs', None, 'tp')
- shared_gate_ready: bfloat16 [2048, 1024], P(None, 'tp')
- shared_up_ready: bfloat16 [2048, 1024], P(None, 'tp')
- shared_down_ready: bfloat16 [1024, 2048], P(None, 'tp')
- mixed: bfloat16 [1536, 2048], P('fs', 'tp')
Inputs may be any that keep to these rules, and one draw needn't show every extreme that they name: `expert_ids`: each row names 8 different experts. Among the 192 rows of one index of fs no expert is named more than 192 times, and in every draw some expert is named exactly 192 times there.
All inputs are finite; a program needn't handle non-finite values.
Results may differ from a plain program's by a relative error of at most 0.0085.
Values may be sent and summed in bfloat16 or wider, within the bound.
No kernel may reach another device: no remote copies, remote signals or barrier semaphores. Data moves between devices by JAX's collectives and lax.ppermute only.
A program may use at most 128 MiB of HBM per device.

v0:
```python
import jax
import jax.numpy as jnp
from jax import lax
from jax.sharding import PartitionSpec as P

TOP_K = 8


EPS = 1e-06


def expert_hidden(rows, gate_new, up_new):
    first = jnp.einsum("secn,enf->secf", rows, gate_new, preferred_element_type=jnp.float32)
    second = jnp.einsum("secn,enf->secf", rows, up_new, preferred_element_type=jnp.float32)
    return (jax.nn.silu(first) * second).astype(jnp.bfloat16)


def body(
    tokens,
    norm_gain,
    expert_gate,
    expert_up,
    expert_down,
    shared_gate,
    shared_up,
    shared_down,
    expert_ids,
    route_weights,
):
    groups = lax.axis_size("fs")
    experts = expert_gate.shape[0]
    per_group = experts // groups
    tok_count = tokens.shape[0]
    capacity = 2 * tok_count * TOP_K // experts
    gate_local = (expert_gate * norm_gain[None, :, None]).astype(jnp.bfloat16)
    up_local = (expert_up * norm_gain[None, :, None]).astype(jnp.bfloat16)
    down_local = expert_down.astype(jnp.bfloat16)
    gate_local = gate_local.reshape((groups, per_group) + gate_local.shape[1:])
    up_local = up_local.reshape((groups, per_group) + up_local.shape[1:])
    down_local = down_local.reshape((groups, per_group) + down_local.shape[1:])
    shared_first_local = (shared_gate * norm_gain[:, None]).astype(jnp.bfloat16)
    shared_second_local = (shared_up * norm_gain[:, None]).astype(jnp.bfloat16)
    shared_third_local = shared_down.astype(jnp.bfloat16)
    gate_moved, up_moved, down_moved = (
        lax.all_to_all(gate_local, "fs", split_axis=0, concat_axis=2, tiled=True),
        lax.all_to_all(up_local, "fs", split_axis=0, concat_axis=2, tiled=True),
        lax.all_to_all(down_local, "fs", split_axis=0, concat_axis=2, tiled=True),
    )
    down_ready = down_moved[0]
    gate_ready = gate_moved[0]
    up_ready = up_moved[0]
    shared_gate_ready, shared_up_ready, shared_down_ready = (
        lax.all_gather(shared_first_local, "fs", axis=0, tiled=True),
        lax.all_gather(shared_second_local, "fs", axis=0, tiled=True),
        lax.all_gather(shared_third_local, "fs", axis=0, tiled=True),
    )
    wide = tokens.astype(jnp.float32)
    normed = (wide * lax.rsqrt(jnp.mean(wide * wide, axis=-1, keepdims=True) + EPS)).astype(
        jnp.bfloat16
    )
    chosen = expert_ids.reshape(-1)
    onehot = (chosen[:, None] == jnp.arange(experts, dtype=jnp.int32)[None, :]).astype(jnp.int32)
    ranks = jnp.sum(jnp.cumsum(onehot, axis=0) * onehot, axis=1) - 1
    owners = jnp.arange(tok_count * TOP_K, dtype=jnp.int32) // TOP_K
    slot_token = jnp.zeros((experts, capacity), jnp.int32).at[chosen, ranks].set(owners)
    outgoing = normed[slot_token.reshape(-1)].reshape(groups, per_group, capacity, normed.shape[1])
    share = capacity // lax.axis_size("tp")
    mine = lax.dynamic_slice_in_dim(outgoing, lax.axis_index("tp") * share, share, 2)
    arrived = lax.all_to_all(mine, "fs", split_axis=0, concat_axis=0, tiled=True)
    hidden = expert_hidden(lax.all_gather(arrived, "tp", axis=2, tiled=True), gate_ready, up_ready)
    shared_first = jnp.dot(normed, shared_gate_ready, preferred_element_type=jnp.float32)
    shared_second = jnp.dot(normed, shared_up_ready, preferred_element_type=jnp.float32)
    shared_hidden = (jax.nn.silu(shared_first) * shared_second).astype(jnp.bfloat16)[None, None]
    columns = down_ready.shape[2]
    routed_piece = lax.all_gather(hidden, "tp", axis=3, tiled=True)
    shared_piece = lax.all_gather(shared_hidden, "tp", axis=3, tiled=True)
    routed_total = jnp.einsum(
        "secf,efd->secd", routed_piece, down_ready, preferred_element_type=jnp.float32
    )
    shared_total = jnp.einsum(
        "abtf,fd->abtd", shared_piece, shared_down_ready, preferred_element_type=jnp.float32
    )
    returned = lax.all_to_all(
        routed_total.astype(jnp.bfloat16), "fs", split_axis=0, concat_axis=0, tiled=True
    )
    returned = returned.reshape(experts * capacity, columns)
    picked = (
        returned[chosen * capacity + ranks].astype(jnp.float32).reshape(tok_count, TOP_K, columns)
    )
    routed = jnp.sum(picked * route_weights[:, :, None], axis=1)
    mixed = (shared_total[0, 0] + routed).astype(jnp.bfloat16)
    return (
        gate_ready,
        up_ready,
        down_ready,
        shared_gate_ready,
        shared_up_ready,
        shared_down_ready,
        mixed,
    )


def solution(mesh):
    in_specs = (
        P("fs", None),
        P("fs"),
        P(None, "fs", "tp"),
        P(None, "fs", "tp"),
        P(None, "fs", "tp"),
        P("fs", "tp"),
        P("fs", "tp"),
        P("fs", "tp"),
        P("fs", None),
        P("fs", None),
    )
    out_specs = (
        P("fs", None, "tp"),
        P("fs", None, "tp"),
        P("fs", None, "tp"),
        P(None, "tp"),
        P(None, "tp"),
        P(None, "tp"),
        P("fs", "tp"),
    )
    return jax.shard_map(body, mesh=mesh, in_specs=in_specs, out_specs=out_specs, check_vma=False)
```

profile of v0, /device:TPU:0, one launch (start us, length us, event | category | flops | bytes accessed | tf_op | source)
XLA Modules:
  0.0 497.0 jit_solution(2639579314955655881)
XLA Ops:
  7.2 0.0 all-gather.13.cloned.1.call-start
  7.2 0.8 copy.33
  8.0 0.1 eq.29
  8.1 0.1 eq.25
  8.2 0.1 reshape.181
  8.4 4.5 reduce-window.6
  12.9 0.4 slice_reduce_fusion
  13.4 0.2 reduce-window.9
  13.5 0.1 broadcast_add_fusion
  13.7 0.7 multiply_reduce_fusion
  14.5 0.8 and_reduce_fusion
  15.3 6.2 %scatter_custom_fusion = s32[3072]{0:T(1024)S(1)} fusion(s32[1536]{0:T(1024)S(1)} %get-tuple-element.17, s32[1536]{0:T(1024)S(1)} %get-tuple-element.16, s32[]{:T(128)} %constant.45.clone.1), kind=kCustom, calls=%fused_computation.50 | custom fusion | bytes 12292
  21.5 1.4 fusion.5
  22.9 1.3 fusion.6
  24.2 15.9 %gather_fusion = bf16[3072,2048]{1,0:T(8,128)(2,1)} fusion(bf16[192,2048]{1,0:T(8,128)(2,1)S(1)} %fusion.6, s32[3072]{0:T(1024)S(1)} %broadcast_clamp_fusion), kind=kCustom, calls=%fused_computation | custom fusion | bytes 25178112 | tf_op jit(solution)/shard_map/gather | solution.py:66
  40.1 2.3 constant_dynamic-slice_fusion
  42.4 77.8 %all_to_all.55 = bf16[8,2,48,2048]{3,2,1,0:T(8,128)(2,1)S(1)} all-to-all(bf16[8,2,48,2048]{3,2,1,0:T(8,128)(2,1)S(1)} %constant_dynamic-slice_fusion), channel_id=1, replica_groups=mesh['fs'=8,'tp'=4] {'fs'}, dimensions={0} | all-to-all | bytes 6291456 | tf_op jit(solution)/shard_map/all_to_all | solution.py:69
  120.2 2.1 copy.36
  122.3 0.0 all-gather.13.cloned.1.call-update
  122.3 0.7 copy-done.8
  123.0 5.8 %multiply_convert_fusion = (bf16[16,256,256]{2,1,0:T(8,128)(2,1)S(1)}, bf16[16,256,256]{2,1,0:T(8,128)(2,1)}) fusion(f32[16,256,256]{2,1,0:T(8,128)} %param.13, f32[256]{0:T(256)S(1)} %copy-done.8, f32[16,256,256]{2,1,0:T(8,128)} %param.12), kind=kLoop, calls=%fused_computation.3 | loop fusion | flops 4194304 | bytes 12583936 | tf_op jit(solution)/shard_map/convert_element_type | solution.py:36
  128.8 51.5 %all_to_all.56 = bf16[8,2,256,256]{3,2,1,0:T(8,128)(2,1)} all-to-all(bf16[8,2,256,256]{3,2,1,0:T(8,128)(2,1)S(1)} %bitcast.80), channel_id=1, replica_groups=mesh['fs'=8,'tp'=4] {'fs'}, dimensions={0} | all-to-all | bytes 4194304 | tf_op jit(solution)/shard_map/all_to_all | solution.py:46
  180.2 3.6 all-to-all-start
  183.8 0.2 all-gather.15.cloned.1.call-start
  184.1 3.1 copy.31
  187.2 44.4 %all-to-all-done = bf16[8,2,256,256]{3,2,1,0:T(8,128)(2,1)S(1)} async-done(((bf16[8,2,256,256]{3,2,1,0:T(8,128)(2,1)}), bf16[8,2,256,256]{3,2,1,0:T(8,128)(2,1)S(1)}, u32[]{:S(2)}, u32[]{:S(2)}) %all-to-all-start) | async-done | bytes 2097184 | tf_op jit(solution)/shard_map/all_to_all | solution.py:45
  231.6 1.5 copy.30
  233.0 10.4 %fusion.19 = f32[2,256,8,192]{1,3,2,0:T(8,128)} fusion(bf16[2,2048,256,1]{2,1,3,0:T(8,128)(2,1)} %bitcast.84, bf16[8,2,192,2048]{3,2,0,1:T(8,128)(2,1)} %all-gather.13.cloned.1.call-done), kind=kOutput, calls=%fused_computation.58 | convolution fusion | flops 3221225472 | bytes 17825792 | tf_op jit(solution)/shard_map/secn,enf->secf/dot_general | solution.py:14
  243.5 0.0 copy-done.2
  243.5 10.5 %fusion.1 = bf16[8,2,192,256]{3,2,0,1:T(8,128)(2,1)} fusion(f32[2,256,8,192]{1,3,2,0:T(8,128)} %fusion.19, bf16[2,2048,256,1]{2,1,3,0:T(8,128)(2,1)S(1)} %bitcast.87, bf16[8,2,192,2048]{3,2,0,1:T(8,128)(2,1)} %all-gather.13.cloned.1.call-done), kind=kOutput, calls=%fused_computation.8 | convolution fusion | flops 3225944064 | bytes 19398656 | tf_op jit(solution)/shard_map/secn,enf->secf/dot_general | solution.py:13
  254.0 0.0 all-gather.15.cloned.1.call-update
  254.0 3.8 convert_element_type.53
  257.8 3.8 all-to-all-start.2
  261.6 0.0 all-gather.7.cloned.1.call-start
  261.7 0.8 multiply_convert_fusion.2
  262.5 0.0 all-gather.7.cloned.1.call-update
  262.5 47.5 %all-to-all-done.2 = bf16[8,2,128,512]{3,2,1,0:T(8,128)(2,1)S(1)} async-done(((bf16[8,2,128,512]{3,2,1,0:T(8,128)(2,1)}), bf16[8,2,128,512]{3,2,1,0:T(8,128)(2,1)S(1)}, u32[]{:S(2)}, u32[]{:S(2)}) %all-to-all-start.2) | async-done | bytes 2097184 | tf_op jit(solution)/shard_map/all_to_all | solution.py:47
  310.0 1.5 copy.32
  311.5 6.8 %convert_bitcast_fusion = bf16[8,2,192,512]{3,2,0,1:T(8,128)(2,1)S(1)} fusion(bf16[8,2,192,1024]{3,2,0,1:T(8,128)(2,1)} %all-gather.15.cloned.1.call-done, bf16[2,1024,512,1]{2,1,3,0:T(8,128)(2,1)} %bitcast.88), kind=kOutput, calls=%fused_computation.14 | convolution fusion | flops 3222798336 | bytes 11534336 | tf_op jit(solution)/shard_map/secf,efd->secd/dot_general | solution.py:77
  318.4 1.9 copy.37
  320.3 4.6 all-to-all-start.4
  324.8 0.0 all-gather.9.cloned.1.call-start
  324.9 0.5 all-gather.9.cloned.1.call-update
  325.4 0.3 all-gather.11.cloned.1.call-start
  325.7 0.7 convert_element_type.56
  326.4 0.0 all-gather.11.cloned.1.call-update
  326.4 0.0 copy-done.7
  326.4 0.1 copy.38
  326.5 31.2 %all-gather.7.cloned.1.call-done = bf16[2048,256]{1,0:T(8,128)(2,1)} async-done(((bf16[256,256]{1,0:T(8,128)(2,1)}), bf16[2048,256]{1,0:T(8,128)(2,1)}) %all-gather.7.cloned.1.call-update) | async-done | bytes 1048592 | tf_op jit(solution)/shard_map/all_gather | solution.py:53
  357.7 69.3 %all-gather.9.cloned.1.call-done = bf16[2048,256]{1,0:T(8,128)(2,1)} async-done(((bf16[256,256]{1,0:T(8,128)(2,1)}), bf16[2048,256]{1,0:T(8,128)(2,1)}) %all-gather.9.cloned.1.call-update) | async-done | bytes 1048592 | tf_op jit(solution)/shard_map/all_gather | solution.py:54
  427.0 41.6 %all-gather.11.cloned.1.call-done = bf16[1024,512]{1,0:T(8,128)(2,1)} async-done(((bf16[128,512]{1,0:T(8,128)(2,1)}), bf16[1024,512]{1,0:T(8,128)(2,1)}) %all-gather.11.cloned.1.call-update) | async-done | bytes 1048592 | tf_op jit(solution)/shard_map/all_gather | solution.py:55
  468.5 1.6 fusion.18
  470.1 1.6 fusion.8
  471.8 6.4 %all-gather = bf16[192,1024]{1,0:T(8,128)(2,1)S(1)} all-gather(bf16[192,256]{1,0:T(8,128)(2,1)S(1)} %fusion.8), channel_id=2, replica_groups=mesh['fs'=8,'tp'=4] {'tp'}, dimensions={1}, use_global_device_ids=true | all-gather | bytes 491520 | tf_op jit(solution)/shard_map/all_gather | solution.py:76
  478.2 0.0 all-to-all-done.4
  478.2 7.2 %gather_fusion.1 = bf16[1536,512]{1,0:T(8,128)(2,1)S(1)} fusion(bf16[3072,512]{1,0:T(8,128)(2,1)} %bitcast.25, s32[2048]{0:T(1024)S(1)} %pad_clamp_fusion), kind=kCustom, calls=%fused_computation.1 | custom fusion | bytes 3151872 | tf_op jit(solution)/shard_map/gather | solution.py:88
  485.5 0.0 copy-start
  485.5 0.0 copy-start.3
  485.5 1.0 fusion
  486.5 0.0 copy-done.1
  486.5 1.1 fusion.7
  487.5 1.0 copy.47
  488.5 1.0 copy.48
  489.5 1.0 copy.49
  (23 shorter events, 0.2 us)
Async XLA Ops:
  7.2 225.9 %all-gather.13.cloned.1.call-start = ((), (), s32[]{:S(2)}) async-start(), calls=%async_computation.8 | async-start | bytes 15728640 | tf_op jit(solution)/shard_map/all_gather | solution.py:70
  122.3 0.7 copy-start.8
  180.2 51.3 %all-to-all-start = ((bf16[8,2,256,256]{3,2,1,0:T(8,128)(2,1)}), bf16[8,2,256,256]{3,2,1,0:T(8,128)(2,1)S(1)}, u32[]{:S(2)}, u32[]{:S(2)}) async-start(bf16[8,2,256,256]{3,2,1,0:T(8,128)(2,1)} %bitcast), calls=%async_computation | async-start | bytes 4194304 | tf_op jit(solution)/shard_map/all_to_all | solution.py:45
  183.8 127.7 %all-gather.15.cloned.1.call-start = ((), (), s32[]{:S(2)}) async-start(), calls=%async_computation.9 | async-start | bytes 7864320 | tf_op jit(solution)/shard_map/all_gather | solution.py:75
  233.0 10.4 %copy-start.2 = (bf16[1,2,8,256,256]{4,3,2,1,0:T(8,128)(2,1)S(1)}, bf16[1,2,8,256,256]{4,3,2,1,0:T(8,128)(2,1)}, u32[]{:S(2)}) copy-start(bf16[1,2,8,256,256]{4,3,2,1,0:T(8,128)(2,1)} %copy.30) | copy-start | bytes 6291460
  257.8 3.8 copy-start.5
  257.8 3.8 copy-start.6
  257.8 52.2 %all-to-all-start.2 = ((bf16[8,2,128,512]{3,2,1,0:T(8,128)(2,1)}), bf16[8,2,128,512]{3,2,1,0:T(8,128)(2,1)S(1)}, u32[]{:S(2)}, u32[]{:S(2)}) async-start(bf16[8,2,128,512]{3,2,1,0:T(8,128)(2,1)} %bitcast.8), calls=%async_computation.2 | async-start | bytes 4194304 | tf_op jit(solution)/shard_map/all_to_all | solution.py:47
  261.6 96.1 %all-gather.7.cloned.1.call-start = ((), (), s32[]{:S(2)}) async-start(), calls=%async_computation.5 | async-start | bytes 1179648 | tf_op jit(solution)/shard_map/all_gather | solution.py:53
  320.2 5.4 %copy-start.4 = (f32[128,512]{1,0:T(8,128)S(1)}, f32[128,512]{1,0:T(8,128)}, u32[]{:S(2)}) copy-start(f32[128,512]{1,0:T(8,128)} %param.17) | copy-start | bytes 786436
  320.3 6.2 %copy-start.7 = (f32[192,8]{0,1:T(8,128)S(1)}, f32[192,8]{0,1:T(8,128)}, u32[]{:S(2)}) copy-start(f32[192,8]{0,1:T(8,128)} %param.19) | copy-start | bytes 18436
  320.3 157.9 %all-to-all-start.4 = ((bf16[8,2,192,512]{3,2,1,0:T(8,128)(2,1)}), bf16[8,2,192,512]{3,2,1,0:T(8,128)(2,1)}, u32[]{:S(2)}, u32[]{:S(2)}) async-start(bf16[8,2,192,512]{3,2,1,0:T(8,128)(2,1)} %copy.37), calls=%async_computation.4 | async-start | bytes 6291456 | tf_op jit(solution)/shard_map/all_to_all | solution.py:83
  324.8 102.1 %all-gather.9.cloned.1.call-start = ((), (), s32[]{:S(2)}) async-start(), calls=%async_computation.6 | async-start | bytes 1179648 | tf_op jit(solution)/shard_map/all_gather | solution.py:54
  325.4 143.1 %all-gather.11.cloned.1.call-start = ((), (), s32[]{:S(2)}) async-start(), calls=%async_computation.7 | async-start | bytes 1179648 | tf_op jit(solution)/shard_map/all_gather | solution.py:55
  478.2 8.3 %copy-start.1 = (bf16[1024,512]{1,0:T(8,128)(2,1)S(1)}, bf16[1024,512]{1,0:T(8,128)(2,1)}, u32[]{:S(2)}) copy-start(bf16[1024,512]{1,0:T(8,128)(2,1)} %all-gather.11.cloned.1.call-done) | copy-start | bytes 3145732
  485.5 2.1 copy-start
  485.5 3.0 copy-start.3
Sparse Core Ops, SparseCore 0:
  122.4 81.1 all-gather.12
  254.1 46.2 all-gather.14
  303.1 54.5 all-gather.6
  360.2 66.6 all-gather.8
  429.5 38.9 all-gather.10
where the time goes:
time: 498 us; the launch traced here: 497 us
  waiting for transfers between devices  234 us (47%)
  blocking collectives  136 us (27%)
  local copies, waits for them, and re-layouts  46.9 us (9%)
  matrix products  32 us (6%)
  other arithmetic  21.2 us (4%)
  between operations  14 us (3%)
  starting transfers between devices  12.6 us (3%)
    all_to_all x1, blocking collectives, body(): lax.all_to_all(mine, 'fs', split_axis=0, concat_axis=0, tiled=True)  77.8 us
    all_gather x1, waiting for transfers between devices, body(): lax.all_gather(shared_second_local, 'fs', axis=0, tiled=True)  69.3 us
    all_to_all x1, blocking collectives, body(): lax.all_to_all(up_local, 'fs', split_axis=0, concat_axis=2, tiled=True)  51.5 us
    all_to_all x1, waiting for transfers between devices, body(): lax.all_to_all(down_local, 'fs', split_axis=0, concat_axis=2, tiled=True)  47.5 us
    all_to_all x1, waiting for transfers between devices, body(): lax.all_to_all(gate_local, 'fs', split_axis=0, concat_axis=2, tiled=True)  44.4 us
    all_gather x1, waiting for transfers between devices, body(): lax.all_gather(shared_third_local, 'fs', axis=0, tiled=True)  41.6 us
    all_gather x1, waiting for transfers between devices, body(): lax.all_gather(shared_first_local, 'fs', axis=0, tiled=True)  31.2 us
    gather x1, local copies, waits for them, and re-layouts, body(): normed[slot_token.reshape(-1)]  15.9 us
  transfers between devices with their start and end apart: 8, of which 5 were waited for; matrix products, arithmetic and copies ran while one was open for 6% of the time, Pallas kernels for 0%

commit v1 on v0

v1 whole, which is shorter than its diff:
```python
import jax
import jax.numpy as jnp
from jax import lax
from jax.sharding import PartitionSpec as P


EPS = 1e-06
LANES = 128


def layer(
    tokens,
    norm_gain,
    expert_gate,
    expert_up,
    expert_down,
    shared_gate,
    shared_up,
    shared_down,
    expert_ids,
    route_weights,
):
    groups = lax.axis_size("fs")
    tp = lax.axis_size("tp")
    experts = expert_gate.shape[0]
    per_group = experts // groups
    tok_count, width = tokens.shape
    bf16, f32 = jnp.bfloat16, jnp.float32

    wide = tokens.astype(f32)
    normed = (wide * lax.rsqrt(jnp.mean(wide * wide, axis=-1, keepdims=True) + EPS)).astype(bf16)
    chosen = expert_ids[:, :, None] == jnp.arange(experts, dtype=jnp.int32)[None, None, :]
    dense = jnp.sum(jnp.where(chosen, route_weights[:, :, None], 0.0), axis=1)
    high = lax.reduce_precision(dense, 8, 7)
    low = (dense - high).astype(bf16)
    columns = jnp.concatenate([high.astype(bf16), low], axis=1)
    columns = jnp.pad(columns, ((0, 0), (0, -columns.shape[1] % LANES)))
    share = tok_count // tp
    rows = jnp.concatenate([normed, columns], axis=1)
    mine = lax.dynamic_slice_in_dim(rows, lax.axis_index("tp") * share, share, 0)
    everyone = lax.all_gather(mine, ("fs", "tp"), axis=0, tiled=True)
    all_tokens = everyone[:, :width]
    own = lax.axis_index("fs") * per_group
    weight = lax.dynamic_slice_in_dim(
        everyone[:, width : width + experts].astype(f32)
        + everyone[:, width + experts : width + 2 * experts].astype(f32),
        own,
        per_group,
        1,
    )

    sg = (shared_gate * norm_gain[:, None]).astype(bf16)
    su = (shared_up * norm_gain[:, None]).astype(bf16)
    sd = shared_down.astype(bf16)
    part = sg.shape[1]
    stacked = jnp.concatenate([jnp.concatenate([sg, su], axis=1), sd], axis=0)
    gathered = lax.all_gather(stacked, "fs", axis=0)
    head = sg.shape[0]
    shared_gate_ready = gathered[:, :head, :part].reshape(groups * head, part)
    shared_up_ready = gathered[:, :head, part:].reshape(groups * head, part)
    shared_down_ready = gathered[:, head:, :].reshape(groups * sd.shape[0], sd.shape[1])

    def moved(local):
        local = local.reshape((groups, per_group) + local.shape[1:])
        return lax.all_to_all(local, "fs", split_axis=0, concat_axis=2, tiled=True)[0]

    gate_ready = moved((expert_gate * norm_gain[None, :, None]).astype(bf16))
    up_ready = moved((expert_up * norm_gain[None, :, None]).astype(bf16))
    down_ready = moved(expert_down.astype(bf16))

    first = jnp.einsum("td,edf->etf", all_tokens, gate_ready, preferred_element_type=f32)
    second = jnp.einsum("td,edf->etf", all_tokens, up_ready, preferred_element_type=f32)
    hidden = (jax.nn.silu(first) * second * weight.T[:, :, None]).astype(bf16)
    routed_hidden = lax.all_gather(hidden, "tp", axis=2, tiled=True)
    partial = jnp.einsum("etf,efd->td", routed_hidden, down_ready, preferred_element_type=f32)
    partial = partial.astype(bf16).reshape(groups, tok_count, partial.shape[1])
    returned = lax.all_to_all(partial, "fs", split_axis=0, concat_axis=0, tiled=True)

    shared_first = jnp.dot(normed, shared_gate_ready, preferred_element_type=f32)
    shared_second = jnp.dot(normed, shared_up_ready, preferred_element_type=f32)
    shared_hidden = (jax.nn.silu(shared_first) * shared_second).astype(bf16)
    shared_piece = lax.all_gather(shared_hidden, "tp", axis=1, tiled=True)
    shared_total = jnp.dot(shared_piece, shared_down_ready, preferred_element_type=f32)
    mixed = (shared_total + jnp.sum(returned.astype(f32), axis=0)).astype(bf16)
    return (
        gate_ready,
        up_ready,
        down_ready,
        shared_gate_ready,
        shared_up_ready,
        shared_down_ready,
        mixed,
    )


def solution(mesh):
    in_specs = (
        P("fs", None),
        P("fs"),
        P(None, "fs", "tp"),
        P(None, "fs", "tp"),
        P(None, "fs", "tp"),
        P("fs", "tp"),
        P("fs", "tp"),
        P("fs", "tp"),
        P("fs", None),
        P("fs", None),
    )
    out_specs = (
        P("fs", None, "tp"),
        P("fs", None, "tp"),
        P("fs", None, "tp"),
        P(None, "tp"),
        P(None, "tp"),
        P(None, "tp"),
        P("fs", "tp"),
    )
    return jax.shard_map(layer, mesh=mesh, in_specs=in_specs, out_specs=out_specs, check_vma=False)
```

time: 498 us -> 332 us (0.67)
  waiting for transfers between devices: 234 us -> 147 us
  blocking collectives: 136 us -> 91.6 us
  local copies, waits for them, and re-layouts: 46.9 us -> 23.1 us
  matrix products: 32 us -> 23.3 us
    all_gather x5 -> x3, waiting for transfers between devices: 142 us -> 59.2 us  [the longest x1 59.2 us: layer(): gathered = lax.all_gather(stacked, 'fs', axis=0)]
    all_to_all x2 -> x1, blocking collectives: 129 us -> 85.1 us  [moved(): lax.all_to_all(local, 'fs', split_axis=0, concat_axis=2, tiled=True)[0]]
    gather x2 -> x0, local copies, waits for them, and re-layouts: 23.1 us -> none  [the longest x1 15.9 us: body(): normed[slot_token.reshape(-1)]]
    dot_general x6, matrix products: 32 us -> 23.3 us  [the longest x1 8.03 us: layer(): jnp.einsum('etf,efd->td', routed_hidden, down_ready, preferred_element_ty...]
    unnamed x24 -> x15, local copies, waits for them, and re-layouts: 10.7 us -> 2.68 us
  transfers between devices with their start and end apart: 8 -> 6, of which waited for: 5 -> 3; matrix products, arithmetic and copies ran while one was open for 6% -> 12% of each run, Pallas kernels for 0% -> 0%
where the time goes in v1:
time: 332 us; the launch traced here: 331 us
  waiting for transfers between devices  147 us (44%)
  blocking collectives  91.6 us (28%)
  matrix products  23.3 us (7%)
  local copies, waits for them, and re-layouts  23.1 us (7%)
  other arithmetic  18.5 us (6%)
  between operations  14 us (4%)
  starting transfers between devices  13.5 us (4%)
    all_to_all x2, waiting for transfers between devices, moved(): lax.all_to_all(local, 'fs', split_axis=0, concat_axis=2, tiled=True)[0]  88 us
    all_to_all x1, blocking collectives, moved(): lax.all_to_all(local, 'fs', split_axis=0, concat_axis=2, tiled=True)[0]  85.1 us
    all_gather x1, waiting for transfers between devices, layer(): gathered = lax.all_gather(stacked, 'fs', axis=0)  59.2 us
    all_to_all x2, starting transfers between devices, moved(): lax.all_to_all(local, 'fs', split_axis=0, concat_axis=2, tiled=True)[0]  8.86 us
    all_to_all x3, local copies, waits for them, and re-layouts, moved(): lax.all_to_all(local, 'fs', split_axis=0, concat_axis=2, tiled=True)[0]  8.76 us
    dot_general x1, matrix products, layer(): jnp.einsum('etf,efd->td', routed_hidden, down_ready, preferred_element_ty...  8.03 us
    dot_general x1, matrix products, layer(): jnp.einsum('td,edf->etf', all_tokens, up_ready, preferred_element_type=f32)  7.72 us
  transfers between devices with their start and end apart: 6, of which 3 were waited for; matrix products, arithmetic and copies ran while one was open for 12% of the time, Pallas kernels for 0%

profile of v1, /device:TPU:0, one launch (start us, length us, event | category | flops | bytes accessed | tf_op | source)
XLA Modules:
  0.0 331.3 jit_solution(6022834244186023149)
XLA Ops:
  7.2 0.0 copy-start.6
  7.2 0.0 all-gather.5.cloned.1.call-start
  7.2 1.4 fusion.8
  8.6 1.3 fusion.9
  9.9 0.7 select_reduce_fusion
  10.7 0.1 copy.49
  10.8 0.7 fusion.13
  11.5 0.0 all-gather.5.cloned.1.call-update
  11.6 0.0 copy-done.6
  11.6 5.8 %multiply_convert_fusion = (bf16[16,256,256]{2,1,0:T(8,128)(2,1)}, bf16[16,256,256]{2,1,0:T(8,128)(2,1)S(1)}) fusion(f32[16,256,256]{2,1,0:T(8,128)} %param.13, f32[256]{0:T(256)S(1)} %copy-done.6, f32[16,256,256]{2,1,0:T(8,128)} %param.12), kind=kLoop, calls=%fused_computation.3 | loop fusion | flops 4194304 | bytes 12583936 | tf_op jit(solution)/shard_map/convert_element_type | solution.py:68
  17.4 2.4 copy.45
  19.7 85.1 %all_to_all.50 = bf16[8,2,256,256]{2,3,1,0:T(8,128)(2,1)S(1)} all-to-all(bf16[8,2,256,256]{2,3,1,0:T(8,128)(2,1)} %bitcast.65), channel_id=1, replica_groups=mesh['fs'=8,'tp'=4] {'fs'}, dimensions={0} | all-to-all | bytes 4194304 | tf_op jit(solution)/shard_map/all_to_all | solution.py:65
  104.9 4.3 %all-to-all-start.1 = ((bf16[8,2,256,256]{3,2,1,0:T(8,128)(2,1)}), bf16[8,2,256,256]{3,2,1,0:T(8,128)(2,1)}, u32[]{:S(2)}, u32[]{:S(2)}) async-start(bf16[8,2,256,256]{3,2,1,0:T(8,128)(2,1)} %bitcast.3), calls=%async_computation.1 | async-start | bytes 4194304 | tf_op jit(solution)/shard_map/all_to_all | solution.py:65
  109.2 0.0 all-gather.7.cloned.1.call-start
  109.3 2.5 copy.46
  111.8 2.9 squeeze.9
  114.7 42.5 %all-to-all-done.1 = bf16[8,2,256,256]{3,2,1,0:T(8,128)(2,1)} async-done(((bf16[8,2,256,256]{3,2,1,0:T(8,128)(2,1)}), bf16[8,2,256,256]{3,2,1,0:T(8,128)(2,1)}, u32[]{:S(2)}, u32[]{:S(2)}) %all-to-all-start.1) | async-done | bytes 2097184 | tf_op jit(solution)/shard_map/all_to_all | solution.py:65
  157.2 3.1 copy.47
  160.3 0.0 all-gather.5.cloned.1.call-done
  160.3 1.5 fusion.15
  161.8 1.2 add_bitcast_fusion
  162.9 1.4 copy.51
  164.3 0.0 copy-start.2
  164.3 5.8 %fusion.2 = f32[2,1536,256]{1,2,0:T(8,128)S(1)} fusion(bf16[2,2048,256]{1,2,0:T(8,128)(2,1)S(1)} %squeeze.9, bf16[1536,2176]{1,0:T(8,128)(2,1)} %all-gather.5.cloned.1.call-done), kind=kOutput, calls=%fused_computation.5 | convolution fusion | flops 3221225472 | bytes 11534336 | tf_op jit(solution)/shard_map/td,edf->etf/dot_general | solution.py:71
  170.1 0.0 copy-done.2
  170.1 7.7 %fusion.7 = bf16[2,1536,256]{1,2,0:T(8,128)(2,1)} fusion(bf16[2,2048,256]{2,1,0:T(8,128)(2,1)S(1)} %bitcast.73, bf16[1536,2176]{1,0:T(8,128)(2,1)} %all-gather.5.cloned.1.call-done, f32[2,1536,256]{1,2,0:T(8,128)S(1)} %fusion.2, f32[2,1536]{1,0:T(2,128)S(1)} %copy.51), kind=kOutput, calls=%fused_computation.12 | convolution fusion | flops 3226730496 | bytes 13119488 | tf_op jit(solution)/shard_map/td,edf->etf/dot_general | solution.py:72
  177.8 0.0 all-gather.7.cloned.1.call-update
  177.8 3.8 %convert_element_type.55 = bf16[16,128,512]{2,1,0:T(8,128)(2,1)} convert(f32[16,128,512]{2,1,0:T(8,128)} %param.14) | non-fusion elementwise | flops 1048576 | bytes 6291456 | tf_op jit(solution)/shard_map/convert_element_type | solution.py:69
  181.6 0.0 copy-start.4
  181.6 0.0 copy-start.5
  181.6 4.5 %all-to-all-start.2 = ((bf16[8,2,128,512]{3,2,1,0:T(8,128)(2,1)}), bf16[8,2,128,512]{3,2,1,0:T(8,128)(2,1)}, u32[]{:S(2)}, u32[]{:S(2)}) async-start(bf16[8,2,128,512]{3,2,1,0:T(8,128)(2,1)} %bitcast.7), calls=%async_computation.2 | async-start | bytes 4194304 | tf_op jit(solution)/shard_map/all_to_all | solution.py:65
  186.2 0.2 all-gather.9.cloned.1.call-start
  186.4 0.0 copy-done.4
  186.4 0.0 copy-done.5
  186.4 1.1 multiply_convert_fusion.3
  187.6 0.8 pad_maximum_fusion
  188.3 0.0 all-gather.9.cloned.1.call-update
  188.4 45.5 %all-to-all-done.2 = bf16[8,2,128,512]{3,2,1,0:T(8,128)(2,1)} async-done(((bf16[8,2,128,512]{3,2,1,0:T(8,128)(2,1)}), bf16[8,2,128,512]{3,2,1,0:T(8,128)(2,1)}, u32[]{:S(2)}, u32[]{:S(2)}) %all-to-all-start.2) | async-done | bytes 2097184 | tf_op jit(solution)/shard_map/all_to_all | solution.py:65
  233.9 3.2 copy.48
  237.0 0.0 all-gather.7.cloned.1.call-done
  237.0 8.0 %fusion.6 = bf16[1536,512]{1,0:T(8,128)(2,1)} fusion(bf16[2,1536,1024]{1,2,0:T(8,128)(2,1)} %all-gather.7.cloned.1.call-done, bf16[2,1024,512]{2,1,0:T(8,128)(2,1)} %bitcast.74), kind=kOutput, calls=%fused_computation.11 | convolution fusion | flops 3222011904 | bytes 9961472 | tf_op jit(solution)/shard_map/etf,efd->td/dot_general | solution.py:75
  245.1 4.3 %all-to-all-start.3 = ((bf16[8,192,512]{2,1,0:T(8,128)(2,1)}), bf16[8,192,512]{2,1,0:T(8,128)(2,1)}, u32[]{:S(2)}, u32[]{:S(2)}) async-start(bf16[8,192,512]{2,1,0:T(8,128)(2,1)} %bitcast.76), calls=%async_computation.3 | async-start | bytes 3145728 | tf_op jit(solution)/shard_map/all_to_all | solution.py:77
  249.4 2.5 copy.53
  251.9 59.2 %all-gather.9.cloned.1.call-done = bf16[3072,512]{1,0:T(8,128)(2,1)} async-done(((bf16[384,512]{1,0:T(8,128)(2,1)}), bf16[3072,512]{1,0:T(8,128)(2,1)}) %all-gather.9.cloned.1.call-update) | async-done | bytes 3145744 | tf_op jit(solution)/shard_map/all_gather | solution.py:57
  311.1 1.3 slice.26
  312.4 0.0 copy-start
  312.5 2.1 fusion.16
  314.6 0.0 copy-start.3
  314.6 0.0 copy-start.1
  314.6 0.4 fusion.17
  315.0 0.4 fusion.11
  315.4 0.2 copy-done.3
  315.5 6.5 %all_gather.17 = bf16[192,1024]{1,0:T(8,128)(2,1)S(1)} all-gather(bf16[192,256]{1,0:T(8,128)(2,1)S(1)} %fusion.11), channel_id=1, replica_groups=mesh['fs'=8,'tp'=4] {'tp'}, dimensions={1}, use_global_device_ids=true | all-gather | bytes 491520 | tf_op jit(solution)/shard_map/all_gather | solution.py:82
  322.0 0.0 all-to-all-done.3
  322.0 1.7 convert_reduce_fusion
  323.7 0.0 copy-done.1
  323.7 0.0 copy-done
  323.7 1.1 fusion.10
  (4 shorter events, 0.0 us)
Async XLA Ops:
  7.2 4.4 %copy-start.6 = (f32[256]{0:T(256)S(1)}, f32[256]{0:T(256)}, u32[]{:S(2)}) copy-start(f32[256]{0:T(256)} %param.11) | copy-start | bytes 3076
  7.2 153.1 %all-gather.5.cloned.1.call-start = ((), (), s32[]{:S(2)}) async-start(), calls=%async_computation.4 | async-start | bytes 6893568 | tf_op jit(solution)/shard_map/all_gather | solution.py:41
  104.9 52.3 %all-to-all-start.1 = ((bf16[8,2,256,256]{3,2,1,0:T(8,128)(2,1)}), bf16[8,2,256,256]{3,2,1,0:T(8,128)(2,1)}, u32[]{:S(2)}, u32[]{:S(2)}) async-start(bf16[8,2,256,256]{3,2,1,0:T(8,128)(2,1)} %bitcast.3), calls=%async_computation.1 | async-start | bytes 4194304 | tf_op jit(solution)/shard_map/all_to_all | solution.py:65
  109.2 127.8 %all-gather.7.cloned.1.call-start = ((), (), s32[]{:S(2)}) async-start(), calls=%async_computation.5 | async-start | bytes 7864320 | tf_op jit(solution)/shard_map/all_gather | solution.py:74
  164.3 5.8 %copy-start.2 = (bf16[8,2,256,256]{3,2,0,1:T(8,128)(2,1)S(1)}, bf16[8,2,256,256]{3,2,0,1:T(8,128)(2,1)}, u32[]{:S(2)}) copy-start(bf16[8,2,256,256]{3,2,0,1:T(8,128)(2,1)} %copy.47) | copy-start | bytes 6291460
  181.6 4.8 %copy-start.4 = (f32[128,512]{1,0:T(8,128)S(1)}, f32[128,512]{1,0:T(8,128)}, u32[]{:S(2)}) copy-start(f32[128,512]{1,0:T(8,128)} %param.17) | copy-start | bytes 786436
  181.6 4.8 %copy-start.5 = (f32[256,256]{1,0:T(8,128)S(1)}, f32[256,256]{1,0:T(8,128)}, u32[]{:S(2)}) copy-start(f32[256,256]{1,0:T(8,128)} %param.15) | copy-start | bytes 786436
  181.6 52.2 %all-to-all-start.2 = ((bf16[8,2,128,512]{3,2,1,0:T(8,128)(2,1)}), bf16[8,2,128,512]{3,2,1,0:T(8,128)(2,1)}, u32[]{:S(2)}, u32[]{:S(2)}) async-start(bf16[8,2,128,512]{3,2,1,0:T(8,128)(2,1)} %bitcast.7), calls=%async_computation.2 | async-start | bytes 4194304 | tf_op jit(solution)/shard_map/all_to_all | solution.py:65
  186.2 124.9 %all-gather.9.cloned.1.call-start = ((), (), s32[]{:S(2)}) async-start(), calls=%async_computation.6 | async-start | bytes 3538944 | tf_op jit(solution)/shard_map/all_gather | solution.py:57
  245.1 76.9 %all-to-all-start.3 = ((bf16[8,192,512]{2,1,0:T(8,128)(2,1)}), bf16[8,192,512]{2,1,0:T(8,128)(2,1)}, u32[]{:S(2)}, u32[]{:S(2)}) async-start(bf16[8,192,512]{2,1,0:T(8,128)(2,1)} %bitcast.76), calls=%async_computation.3 | async-start | bytes 3145728 | tf_op jit(solution)/shard_map/all_to_all | solution.py:77
  312.4 11.2 %copy-start = (bf16[8,128,512]{2,1,0:T(8,128)(2,1)}, bf16[8,128,512]{2,1,0:T(8,128)(2,1)S(1)}, u32[]{:S(2)}) copy-start(bf16[8,128,512]{2,1,0:T(8,128)(2,1)S(1)} %slice.26) | copy-start | bytes 3145732
  314.6 1.0 copy-start.3
  314.6 9.1 %copy-start.1 = (bf16[8,256,256]{2,1,0:T(8,128)(2,1)}, bf16[8,256,256]{2,1,0:T(8,128)(2,1)S(1)}, u32[]{:S(2)}) copy-start(bf16[8,256,256]{2,1,0:T(8,128)(2,1)S(1)} %get-tuple-element.38) | copy-start | bytes 3145732
Sparse Core Ops, SparseCore 0:
  11.7 93.7 all-gather.4
  178.0 45.4 all-gather.6
  226.2 84.8 all-gather.8

commit v2 on v1

v2 whole, which is shorter than its diff:
```python
import jax
import jax.numpy as jnp
from jax import lax
from jax.sharding import PartitionSpec as P


EPS = 1e-06
LANES = 128


def layer(
    tokens,
    norm_gain,
    expert_gate,
    expert_up,
    expert_down,
    shared_gate,
    shared_up,
    shared_down,
    expert_ids,
    route_weights,
):
    groups = lax.axis_size("fs")
    tp = lax.axis_size("tp")
    experts = expert_gate.shape[0]
    per_group = experts // groups
    tok_count, width = tokens.shape
    bf16, f32 = jnp.bfloat16, jnp.float32

    def normalised(block):
        wide = block.astype(f32)
        scale = lax.rsqrt(jnp.mean(wide * wide, axis=-1, keepdims=True) + EPS)
        return (wide * scale).astype(bf16)

    chosen = expert_ids[:, :, None] == jnp.arange(experts, dtype=jnp.int32)[None, None, :]
    dense = jnp.sum(jnp.where(chosen, route_weights[:, :, None], 0.0), axis=1)
    high = lax.reduce_precision(dense, 8, 7)
    low = (dense - high).astype(bf16)
    columns = jnp.concatenate([high.astype(bf16), low], axis=1)
    columns = jnp.pad(columns, ((0, 0), (0, -columns.shape[1] % LANES)))
    share = tok_count // tp
    rows = jnp.concatenate([tokens, columns], axis=1)
    mine = lax.dynamic_slice_in_dim(rows, lax.axis_index("tp") * share, share, 0)
    mine = lax.all_gather(mine, "fs", axis=0)
    mine = jnp.concatenate([normalised(mine[:, :, :width]), mine[:, :, width:]], axis=2)
    everyone = lax.all_gather(mine, "tp", axis=1, tiled=True)
    everyone = everyone.reshape(groups * tok_count, everyone.shape[2])
    all_tokens = everyone[:, :width]
    own = lax.axis_index("fs") * per_group
    line = jnp.arange(everyone.shape[1] - width, dtype=jnp.int32)[:, None]
    target = own + jnp.arange(per_group, dtype=jnp.int32)[None, :]
    pick = ((line == target) | (line == target + experts)).astype(bf16)
    weight = jnp.einsum("tc,ce->et", everyone[:, width:], pick, preferred_element_type=f32)

    sg = (shared_gate * norm_gain[:, None]).astype(bf16)
    su = (shared_up * norm_gain[:, None]).astype(bf16)
    sd = shared_down.astype(bf16)
    part = sg.shape[1]
    gathered = lax.all_gather(jnp.concatenate([sg, su], axis=1), "fs", axis=0, tiled=True)
    shared_down_ready = lax.all_gather(sd, "fs", axis=0, tiled=True)
    shared_gate_ready = gathered[:, :part]
    shared_up_ready = gathered[:, part:]

    def moved(local):
        local = local.reshape((groups, per_group) + local.shape[1:])
        return lax.all_to_all(local, "fs", split_axis=0, concat_axis=0, tiled=True)

    def ready(block):
        return block.transpose(1, 0, 2, 3).reshape(per_group, -1, block.shape[3])

    def of(block, e):
        return block[:, e].reshape(-1, block.shape[3])

    gate_local = (expert_gate * norm_gain[None, :, None]).astype(bf16)
    gate_local, expert_up = lax.optimization_barrier((gate_local, expert_up))
    gate_moved = moved(gate_local)
    up_local = (expert_up * norm_gain[None, :, None]).astype(bf16)
    up_moved = moved(up_local)
    down_moved = moved(expert_down.astype(bf16))
    gate_ready, up_ready, down_ready = ready(gate_moved), ready(up_moved), ready(down_moved)

    total = 0.0
    for e in range(per_group):
        gate_e, up_e = of(gate_moved, e), of(up_moved, e)
        first = jnp.dot(all_tokens, gate_e, preferred_element_type=f32)
        second = jnp.dot(all_tokens, up_e, preferred_element_type=f32)
        hidden = (jax.nn.silu(first) * second * weight[e][:, None]).astype(bf16)
        spread = lax.all_gather(hidden, "tp", axis=1, tiled=True)
        total = total + jnp.dot(spread, of(down_moved, e), preferred_element_type=f32)
    partial = total.astype(bf16).reshape(groups, tok_count, total.shape[1])
    returned = lax.all_to_all(partial, "fs", split_axis=0, concat_axis=0, tiled=True)
    returned = jnp.sum(returned.astype(f32), axis=0)

    normed = normalised(tokens)
    shared_first = jnp.dot(normed, shared_gate_ready, preferred_element_type=f32)
    shared_second = jnp.dot(normed, shared_up_ready, preferred_element_type=f32)
    shared_hidden = (jax.nn.silu(shared_first) * shared_second).astype(bf16)
    shared_piece = lax.all_gather(shared_hidden, "tp", axis=1, tiled=True)
    shared_total = jnp.dot(shared_piece, shared_down_ready, preferred_element_type=f32)
    mixed = (shared_total + returned).astype(bf16)
    return (
        gate_ready,
        up_ready,
        down_ready,
        shared_gate_ready,
        shared_up_ready,
        shared_down_ready,
        mixed,
    )


def solution(mesh):
    in_specs = (
        P("fs", None),
        P("fs"),
        P(None, "fs", "tp"),
        P(None, "fs", "tp"),
        P(None, "fs", "tp"),
        P("fs", "tp"),
        P("fs", "tp"),
        P("fs", "tp"),
        P("fs", None),
        P("fs", None),
    )
    out_specs = (
        P("fs", None, "tp"),
        P("fs", None, "tp"),
        P("fs", None, "tp"),
        P(None, "tp"),
        P(None, "tp"),
        P(None, "tp"),
        P("fs", "tp"),
    )
    return jax.shard_map(layer, mesh=mesh, in_specs=in_specs, out_specs=out_specs, check_vma=False)
```

time: 332 us -> 372 us (1.12)
  waiting for transfers between devices: 147 us -> 258 us
  blocking collectives: 91.6 us -> 6.44 us
  matrix products: 23.3 us -> 33.7 us
  local copies, waits for them, and re-layouts: 23.1 us -> 19.2 us
  starting transfers between devices: 13.5 us -> 17.3 us
    all_to_all x1 -> x0, blocking collectives: 85.1 us -> none  [moved(): lax.all_to_all(local, 'fs', split_axis=0, concat_axis=2, tiled=True)[0]]
    all_gather x3 -> x6, waiting for transfers between devices: 59.2 us -> 123 us  [the longest x1 50.3 us: layer(): lax.all_gather(jnp.concatenate([sg, su], axis=1), 'fs', axis=0, tiled=True)]
    all_to_all x2 -> x3, waiting for transfers between devices: 88 us -> 135 us  [moved(): return lax.all_to_all(local, 'fs', split_axis=0, concat_axis=0, tiled=True)]
    dot_general x3 -> x7, matrix products: 21.5 us -> 31.8 us  [the longest x2 11.5 us: layer(): jnp.dot(spread, of(down_moved, e), preferred_element_type=f32)]
    slice x3 -> x6, local copies, waits for them, and re-layouts: 4.92 us -> 9.52 us  [the longest x3 6.88 us: of(): return block[:, e].reshape(-1, block.shape[3])]
    all_to_all x2 -> x3, starting transfers between devices: 8.86 us -> 12.5 us  [moved(): return lax.all_to_all(local, 'fs', split_axis=0, concat_axis=0, tiled=True)]
    convert_element_type x3 -> x4, other arithmetic: 10.9 us -> 13.1 us  [the longest x1 4.99 us: layer(): up_local = (expert_up * norm_gain[None, :, None]).astype(bf16)]
  transfers between devices with their start and end apart: 6 -> 10, of which waited for: 3 -> 6; matrix products, arithmetic and copies ran while one was open for 12% -> 15% of each run, Pallas kernels for 0% -> 0%
where the time goes in v2:
time: 372 us; the launch traced here: 371 us
  waiting for transfers between devices  258 us (69%)
  matrix products  33.7 us (9%)
  other arithmetic  22.1 us (6%)
  local copies, waits for them, and re-layouts  19.2 us (5%)
  starting transfers between devices  17.3 us (5%)
  between operations  14.4 us (4%)
  blocking collectives  6.44 us (2%)
    all_to_all x3, waiting for transfers between devices, moved(): return lax.all_to_all(local, 'fs', split_axis=0, concat_axis=0, tiled=True)  135 us
    all_gather x1, waiting for transfers between devices, layer(): lax.all_gather(jnp.concatenate([sg, su], axis=1), 'fs', axis=0, tiled=True)  50.3 us
    all_gather x1, waiting for transfers between devices, layer(): mine = lax.all_gather(mine, 'fs', axis=0)  48.9 us
    all_gather x1, waiting for transfers between devices, layer(): shared_down_ready = lax.all_gather(sd, 'fs', axis=0, tiled=True)  23.9 us
    all_to_all x3, starting transfers between devices, moved(): return lax.all_to_all(local, 'fs', split_axis=0, concat_axis=0, tiled=True)  12.5 us
    dot_general x2, matrix products, layer(): jnp.dot(spread, of(down_moved, e), preferred_element_type=f32)  11.5 us
    dot_general x2, matrix products, layer(): first = jnp.dot(all_tokens, gate_e, preferred_element_type=f32)  9.73 us
    dot_general x2, matrix products, layer(): second = jnp.dot(all_tokens, up_e, preferred_element_type=f32)  9.19 us
  transfers between devices with their start and end apart: 10, of which 6 were waited for; matrix products, arithmetic and copies ran while one was open for 15% of the time, Pallas kernels for 0%

profile of v2, /device:TPU:0, one launch (start us, length us, event | category | flops | bytes accessed | tf_op | source)
XLA Modules:
  0.0 371.0 jit_solution(1274880108709583326)
XLA Ops:
  7.2 0.0 all-gather.18.cloned.1.call-start
  7.2 0.7 select_reduce_fusion
  8.0 0.1 copy.35
  8.1 1.6 fusion.39
  9.7 0.0 all-gather.18.cloned.1.call-update
  9.8 0.0 all-gather.12.cloned.1.call-start
  9.8 48.9 %all-gather.18.cloned.1.call-done = bf16[384,2176]{1,0:T(8,128)(2,1)} async-done(((bf16[48,2176]{1,0:T(8,128)(2,1)}), bf16[384,2176]{1,0:T(8,128)(2,1)}) %all-gather.18.cloned.1.call-update) | async-done | bytes 1671184 | tf_op jit(solution)/shard_map/all_gather | solution.py:44
  58.7 1.9 fusion.8
  60.6 0.9 slice.59
  61.5 0.3 fusion.9
  61.9 0.0 copy-start.10
  61.9 1.3 pad_maximum_fusion
  63.2 0.0 all-gather.12.cloned.1.call-update
  63.2 4.0 %multiply_convert_fusion.1 = bf16[16,256,256]{2,1,0:T(8,128)(2,1)} fusion(f32[16,256,256]{2,1,0:T(8,128)} %param.12, f32[256]{0:T(256)S(1)} %copy-done.10), kind=kLoop, calls=%fused_computation.1 | loop fusion | flops 2097152 | bytes 6292480 | tf_op jit(solution)/shard_map/convert_element_type | solution.py:74
  67.2 3.6 all-to-all-start
  70.9 5.0 %multiply_convert_fusion = bf16[16,256,256]{2,1,0:T(8,128)(2,1)} fusion(f32[16,256,256]{2,1,0:T(8,128)} %param.13, f32[256]{0:T(256)S(1)} %copy-done.10), kind=kLoop, calls=%fused_computation | loop fusion | flops 2097152 | bytes 6292480 | tf_op jit(solution)/shard_map/convert_element_type | solution.py:77
  75.9 42.4 %all-to-all-done = bf16[8,2,256,256]{3,2,1,0:T(8,128)(2,1)S(1)} async-done(((bf16[8,2,256,256]{3,2,1,0:T(8,128)(2,1)}), bf16[8,2,256,256]{3,2,1,0:T(8,128)(2,1)S(1)}, u32[]{:S(2)}, u32[]{:S(2)}) %all-to-all-start) | async-done | bytes 2097184 | tf_op jit(solution)/shard_map/all_to_all | solution.py:66
  118.3 4.3 %all-to-all-start.1 = ((bf16[8,2,256,256]{3,2,1,0:T(8,128)(2,1)}), bf16[8,2,256,256]{3,2,1,0:T(8,128)(2,1)}, u32[]{:S(2)}, u32[]{:S(2)}) async-start(bf16[8,2,256,256]{3,2,1,0:T(8,128)(2,1)} %bitcast.34), calls=%async_computation.1 | async-start | bytes 4194304 | tf_op jit(solution)/shard_map/all_to_all | solution.py:66
  122.6 0.0 all-gather.14.cloned.1.call-start
  122.7 1.1 fusion.47
  123.8 46.6 %all-to-all-done.1 = bf16[8,2,256,256]{3,2,1,0:T(8,128)(2,1)} async-done(((bf16[8,2,256,256]{3,2,1,0:T(8,128)(2,1)}), bf16[8,2,256,256]{3,2,1,0:T(8,128)(2,1)}, u32[]{:S(2)}, u32[]{:S(2)}) %all-to-all-start.1) | async-done | bytes 2097184 | tf_op jit(solution)/shard_map/all_to_all | solution.py:66
  170.4 3.0 fusion.48
  173.5 1.4 fusion.34
  174.9 0.1 slice_reduce_fusion
  174.9 0.0 copy-start.6
  175.0 5.1 %fusion.6 = f32[1536,256]{1,0:T(8,128)S(1)} fusion(bf16[2048,256]{1,0:T(8,128)(2,1)} %bitcast.45, bf16[1536,2176]{1,0:T(8,128)(2,1)} %bitcast.50), kind=kOutput, calls=%fused_computation.8 | convolution fusion | flops 1610612736 | bytes 8912896 | tf_op jit(solution)/shard_map/dot_general | solution.py:85
  180.1 2.9 fusion.26
  182.9 0.0 all-gather.14.cloned.1.call-update
  183.0 0.0 all-gather.16.cloned.1.call-start
  183.0 0.0 copy-start.3
  183.0 4.7 %fusion.2 = f32[1536,256]{1,0:T(8,128)S(1)} fusion(bf16[2048,256]{1,0:T(8,128)(2,1)S(1)} %bitcast.43, bf16[1536,2176]{1,0:T(8,128)(2,1)} %bitcast.51), kind=kOutput, calls=%fused_computation.4 | convolution fusion | flops 1610612736 | bytes 8912896 | tf_op jit(solution)/shard_map/dot_general | solution.py:85
  187.7 6.3 %fusion.23 = bf16[1536,256]{1,0:T(8,128)(2,1)} fusion(bf16[2048,256]{1,0:T(8,128)(2,1)S(1)} %bitcast.44, bf16[1536,2176]{1,0:T(8,128)(2,1)} %bitcast.52, f32[1536,256]{1,0:T(8,128)S(1)} %fusion.2, f32[1536]{0:T(1024)S(1)} %get-tuple-element.11), kind=kOutput, calls=%fused_computation.21 | convolution fusion | flops 1613365248 | bytes 9705472 | tf_op jit(solution)/shard_map/dot_general | solution.py:86
  194.0 0.0 all-gather.16.cloned.1.call-update
  194.0 3.8 %convert_element_type.59 = bf16[16,128,512]{2,1,0:T(8,128)(2,1)} convert(f32[16,128,512]{2,1,0:T(8,128)} %param.14) | non-fusion elementwise | flops 1048576 | bytes 6291456 | tf_op jit(solution)/shard_map/convert_element_type | solution.py:79
  197.9 4.5 %all-to-all-start.2 = ((bf16[8,2,128,512]{3,2,1,0:T(8,128)(2,1)}), bf16[8,2,128,512]{3,2,1,0:T(8,128)(2,1)}, u32[]{:S(2)}, u32[]{:S(2)}) async-start(bf16[8,2,128,512]{3,2,1,0:T(8,128)(2,1)} %bitcast.33), calls=%async_computation.2 | async-start | bytes 4194304 | tf_op jit(solution)/shard_map/all_to_all | solution.py:66
  202.3 0.0 all-gather.10.cloned.1.call-start
  202.4 0.7 convert_element_type.62
  203.1 0.0 all-gather.10.cloned.1.call-update
  203.1 0.2 all-gather.8.cloned.1.call-start
  203.4 0.1 multiply_convert_fusion.3
  203.5 0.7 pad_maximum_fusion.1
  204.2 0.0 all-gather.8.cloned.1.call-update
  204.2 45.6 %all-to-all-done.2 = bf16[8,2,128,512]{3,2,1,0:T(8,128)(2,1)} async-done(((bf16[8,2,128,512]{3,2,1,0:T(8,128)(2,1)}), bf16[8,2,128,512]{3,2,1,0:T(8,128)(2,1)}, u32[]{:S(2)}, u32[]{:S(2)}) %all-to-all-start.2) | async-done | bytes 2097184 | tf_op jit(solution)/shard_map/all_to_all | solution.py:66
  249.8 2.7 fusion.46
  252.5 5.7 %fusion.50 = f32[1536,512]{1,0:T(8,128)} fusion(bf16[1536,1024]{1,0:T(8,128)(2,1)} %all-gather.14.cloned.1.call-done, bf16[1024,512]{1,0:T(8,128)(2,1)} %bitcast.48), kind=kOutput, calls=%fused_computation.65 | convolution fusion | flops 1610612736 | bytes 7340032 | tf_op jit(solution)/shard_map/dot_general | solution.py:89
  258.2 5.8 %fusion.10 = bf16[1536,512]{1,0:T(8,128)(2,1)} fusion(f32[1536,512]{1,0:T(8,128)} %fusion.50, bf16[1536,1024]{1,0:T(8,128)(2,1)} %all-gather.16.cloned.1.call-done, bf16[1024,512]{1,0:T(8,128)(2,1)S(1)} %bitcast.47), kind=kOutput, calls=%fused_computation.16 | convolution fusion | flops 1612185600 | bytes 8912896 | tf_op jit(solution)/shard_map/dot_general | solution.py:89
  264.0 4.4 %all-to-all-start.3 = ((bf16[8,192,512]{2,1,0:T(8,128)(2,1)}), bf16[8,192,512]{2,1,0:T(8,128)(2,1)}, u32[]{:S(2)}, u32[]{:S(2)}) async-start(bf16[8,192,512]{2,1,0:T(8,128)(2,1)} %bitcast.42), calls=%async_computation.3 | async-start | bytes 3145728 | tf_op jit(solution)/shard_map/all_to_all | solution.py:91
  268.4 0.2 fusion.29
  268.7 23.9 %all-gather.10.cloned.1.call-done = bf16[1024,512]{1,0:T(8,128)(2,1)} async-done(((bf16[128,512]{1,0:T(8,128)(2,1)}), bf16[1024,512]{1,0:T(8,128)(2,1)}) %all-gather.10.cloned.1.call-update) | async-done | bytes 1048592 | tf_op jit(solution)/shard_map/all_gather | solution.py:60
  292.6 1.5 copy.31
  294.1 3.1 copy.32
  297.2 3.1 copy.33
  300.3 50.3 %all-gather.8.cloned.1.call-done = bf16[2048,512]{1,0:T(8,128)(2,1)} async-done(((bf16[256,512]{1,0:T(8,128)(2,1)}), bf16[2048,512]{1,0:T(8,128)(2,1)}) %all-gather.8.cloned.1.call-update) | async-done | bytes 2097168 | tf_op jit(solution)/shard_map/all_gather | solution.py:59
  350.6 1.7 fusion.49
  352.3 0.0 copy-start.5
  352.3 0.0 copy-start.4
  352.3 0.4 fusion.37
  352.7 0.5 copy-done.5
  353.2 0.3 copy-done.4
  353.6 0.4 fusion.32
  354.0 6.4 %all_gather.26 = bf16[192,1024]{1,0:T(8,128)(2,1)S(1)} all-gather(bf16[192,256]{1,0:T(8,128)(2,1)S(1)} %fusion.32), channel_id=1, replica_groups=mesh['fs'=8,'tp'=4] {'tp'}, dimensions={1}, use_global_device_ids=true | all-gather | bytes 491520 | tf_op jit(solution)/shard_map/all_gather | solution.py:98
  360.5 1.7 convert_reduce_fusion
  362.1 1.1 fusion.31
  363.2 1.0 copy.37
  (29 shorter events, 0.1 us)
Async XLA Ops:
  7.2 51.5 %all-gather.18.cloned.1.call-start = ((), (), s32[]{:S(2)}) async-start(), calls=%async_computation.9 | async-start | bytes 1880064 | tf_op jit(solution)/shard_map/all_gather | solution.py:44
  9.8 163.7 %all-gather.12.cloned.1.call-start = ((), (), s32[]{:S(2)}) async-start(), calls=%async_computation.6 | async-start | bytes 8355840 | tf_op jit(solution)/shard_map/all_gather | solution.py:46
  58.7 2.8 copy-start
  61.9 1.4 copy-start.10
  67.2 51.0 %all-to-all-start = ((bf16[8,2,256,256]{3,2,1,0:T(8,128)(2,1)}), bf16[8,2,256,256]{3,2,1,0:T(8,128)(2,1)S(1)}, u32[]{:S(2)}, u32[]{:S(2)}) async-start(bf16[8,2,256,256]{3,2,1,0:T(8,128)(2,1)} %bitcast.35), calls=%async_computation | async-start | bytes 4194304 | tf_op jit(solution)/shard_map/all_to_all | solution.py:66
  118.3 52.2 %all-to-all-start.1 = ((bf16[8,2,256,256]{3,2,1,0:T(8,128)(2,1)}), bf16[8,2,256,256]{3,2,1,0:T(8,128)(2,1)}, u32[]{:S(2)}, u32[]{:S(2)}) async-start(bf16[8,2,256,256]{3,2,1,0:T(8,128)(2,1)} %bitcast.34), calls=%async_computation.1 | async-start | bytes 4194304 | tf_op jit(solution)/shard_map/all_to_all | solution.py:66
  122.6 129.8 %all-gather.14.cloned.1.call-start = ((), (), s32[]{:S(2)}) async-start(), calls=%async_computation.7 | async-start | bytes 3932160 | tf_op jit(solution)/shard_map/all_gather | solution.py:88
  173.5 6.5 %slice-start = ((s8[6684672]{0:T(1024)(128)(4,1)}), s8[4194304]{0:T(1024)(128)(4,1)S(1)}, s32[]{:S(2)}) async-start(s8[6684672]{0:T(1024)(128)(4,1)} %bitcast.53), calls=%async_computation.10 | async-start | bytes 8388608
  174.9 5.1 %copy-start.6 = (bf16[8,1,256,256]{3,2,1,0:T(8,128)(2,1)S(1)}, bf16[8,1,256,256]{3,2,1,0:T(8,128)(2,1)}, u32[]{:S(2)}) copy-start(bf16[8,1,256,256]{3,2,1,0:T(8,128)(2,1)} %get-tuple-element.18) | copy-start | bytes 3145732
  174.9 5.1 %slice-start.1 = ((s8[6684672]{0:T(1024)(128)(4,1)}), s8[2490368]{0:T(1024)(128)(4,1)S(1)}, s32[]{:S(2)}) async-start(s8[6684672]{0:T(1024)(128)(4,1)} %bitcast.53), calls=%async_computation.11 | async-start | bytes 4980736
  183.0 75.2 %all-gather.16.cloned.1.call-start = ((), (), s32[]{:S(2)}) async-start(), calls=%async_computation.8 | async-start | bytes 3932160 | tf_op jit(solution)/shard_map/all_gather | solution.py:88
  183.0 4.7 %copy-start.3 = (bf16[8,1,256,256]{3,2,1,0:T(8,128)(2,1)S(1)}, bf16[8,1,256,256]{3,2,1,0:T(8,128)(2,1)}, u32[]{:S(2)}) copy-start(bf16[8,1,256,256]{3,2,1,0:T(8,128)(2,1)} %get-tuple-element.17) | copy-start | bytes 3145732
  197.8 4.6 %copy-start.7 = (f32[128,512]{1,0:T(8,128)S(1)}, f32[128,512]{1,0:T(8,128)}, u32[]{:S(2)}) copy-start(f32[128,512]{1,0:T(8,128)} %param.17) | copy-start | bytes 786436
  197.8 5.5 %copy-start.8 = (f32[256,256]{1,0:T(8,128)S(1)}, f32[256,256]{1,0:T(8,128)}, u32[]{:S(2)}) copy-start(f32[256,256]{1,0:T(8,128)} %param.15) | copy-start | bytes 786436
  197.8 5.5 %copy-start.9 = (f32[256,256]{1,0:T(8,128)S(1)}, f32[256,256]{1,0:T(8,128)}, u32[]{:S(2)}) copy-start(f32[256,256]{1,0:T(8,128)} %param.16) | copy-start | bytes 786436
  197.9 51.9 %all-to-all-start.2 = ((bf16[8,2,128,512]{3,2,1,0:T(8,128)(2,1)}), bf16[8,2,128,512]{3,2,1,0:T(8,128)(2,1)}, u32[]{:S(2)}, u32[]{:S(2)}) async-start(bf16[8,2,128,512]{3,2,1,0:T(8,128)(2,1)} %bitcast.33), calls=%async_computation.2 | async-start | bytes 4194304 | tf_op jit(solution)/shard_map/all_to_all | solution.py:66
  202.3 90.2 %all-gather.10.cloned.1.call-start = ((), (), s32[]{:S(2)}) async-start(), calls=%async_computation.5 | async-start | bytes 1179648 | tf_op jit(solution)/shard_map/all_gather | solution.py:60
  203.1 147.5 %all-gather.8.cloned.1.call-start = ((), (), s32[]{:S(2)}) async-start(), calls=%async_computation.4 | async-start | bytes 2359296 | tf_op jit(solution)/shard_map/all_gather | solution.py:59
  263.9 4.4 %copy-start.2 = (bf16[192,2048]{1,0:T(8,128)(2,1)S(1)}, bf16[192,2048]{1,0:T(8,128)(2,1)}, u32[]{:S(2)}) copy-start(bf16[192,2048]{1,0:T(8,128)(2,1)} %param.10) | copy-start | bytes 2359300
  264.0 96.5 %all-to-all-start.3 = ((bf16[8,192,512]{2,1,0:T(8,128)(2,1)}), bf16[8,192,512]{2,1,0:T(8,128)(2,1)}, u32[]{:S(2)}, u32[]{:S(2)}) async-start(bf16[8,192,512]{2,1,0:T(8,128)(2,1)} %bitcast.42), calls=%async_computation.3 | async-start | bytes 3145728 | tf_op jit(solution)/shard_map/all_to_all | solution.py:91
  352.3 1.0 copy-start.5
  352.3 1.3 copy-start.4
  353.6 8.5 %copy-start.1 = (bf16[1024,512]{1,0:T(8,128)(2,1)S(1)}, bf16[1024,512]{1,0:T(8,128)(2,1)}, u32[]{:S(2)}) copy-start(bf16[1024,512]{1,0:T(8,128)(2,1)} %all-gather.10.cloned.1.call-done) | copy-start | bytes 3145732
Sparse Core Ops, SparseCore 0:
  10.7 47.9 all-gather.17
  63.3 46.9 all-gather.11
  183.1 27.8 all-gather.13
  212.9 28.8 all-gather.15
  244.4 48.1 all-gather.9
  294.6 55.9 all-gather.7
